TPU v7x, 256 devices: a whole 4x4x8 slice. The times are simulated.
256 devices in a mesh: ep: 64 (over z, x, core), tp: 4 (over y).
Axes of the slice: x: 4, y: 4, z: 8, core: 2. Of those that a mesh axis runs over, the one named last changes fastest.
Arguments:
- tokens: bfloat16 [65536, 2048], P(('ep', 'tp')), may hold values from -6 to 6
- norm_gain: bfloat16 [2048], replicated, may hold values from 0.099609375 to 1.8984375
- expert_ids: int32 [65536, 2], P(('ep', 'tp')), may hold values from 0 to 63, all different within a row; in each aligned block of 256 rows (0 to 255, 256 to 511, ...) at most 16 rows name the same one
- group_weight: float32 [65536], P(('ep', 'tp')), may hold values from 0.25 to 1
- expert_logit: float32 [65536, 2], P(('ep', 'tp')), may hold values from -4 to 4
- w_gate: bfloat16 [64, 2048, 1024], P('ep', None, 'tp'), may hold values from -0.125 to 0.125
- w_up: bfloat16 [64, 2048, 1024], P('ep', None, 'tp'), may hold values from -0.125 to 0.125
- w_down: bfloat16 [64, 1024, 2048], P('ep', 'tp')
- final_gain: bfloat16 [2048], P('tp'), may hold values from 0.099609375 to 1.8984375
Outputs:
- normed_out: bfloat16 [65536, 2048], P('ep', 'tp')
Inputs may be any that keep to these rules, and one draw needn't show every extreme that they name: `expert_ids`: the 2 experts of a token differ. Among the rows of one device (aligned blocks of 256 tokens) no expert is named more than 16 times, a bound that some block reaches.
All inputs are finite; a program needn't handle non-finite values.
Results may differ from a plain program's by a relative error of at most 0.0058.
Values may be sent and summed in bfloat16 or wider, within the bound.
A program may use at most 128 MiB of HBM per device.

v0:
```python
import jax
import jax.numpy as jnp
from jax import lax
from jax.sharding import PartitionSpec as P

D = 2048
CAP = 16
EPS = 1e-06


def local(
    tokens, norm_gain, expert_ids, group_weight, expert_logit, w_gate, w_up, w_down, final_gain
):
    rows, width = tokens.shape
    experts = lax.axis_size("ep")
    slots = experts * CAP
    down_whole = lax.all_gather(w_down, "tp", axis=1, tiled=True)[0]
    both = lax.all_gather(jnp.concatenate((w_gate, w_up), axis=0), "tp", axis=2, tiled=True)
    tokens_f = tokens.astype(jnp.float32)
    inverse_in = lax.rsqrt(jnp.mean(tokens_f * tokens_f, axis=-1, keepdims=True) + EPS)
    normed_in = (tokens_f * inverse_in * norm_gain.astype(jnp.float32)).astype(jnp.bfloat16)
    lane = jnp.arange(experts, dtype=jnp.int32)[None, :]
    first = expert_ids[:, 0:1] == lane
    second = expert_ids[:, 1:2] == lane
    named = (first | second).astype(jnp.bfloat16)
    order = jnp.arange(rows, dtype=jnp.int32)
    earlier = (order[:, None] > order[None, :]).astype(jnp.bfloat16)
    before = jnp.dot(earlier, named, preferred_element_type=jnp.float32)
    rank0 = jnp.sum(jnp.where(first, before, 0.0), axis=1).astype(jnp.int32)
    rank1 = jnp.sum(jnp.where(second, before, 0.0), axis=1).astype(jnp.int32)
    at0 = expert_ids[:, 0] * CAP + rank0
    at1 = expert_ids[:, 1] * CAP + rank1
    slot = jnp.arange(slots, dtype=jnp.int32)
    pick = ((slot[:, None] == at0[None, :]) | (slot[:, None] == at1[None, :])).astype(jnp.bfloat16)
    outgoing = jnp.dot(pick, normed_in, preferred_element_type=jnp.float32).astype(jnp.bfloat16)
    incoming = lax.all_to_all(
        outgoing.reshape(experts, CAP, width), "ep", split_axis=0, concat_axis=0, tiled=True
    )
    routed = incoming.reshape(slots, width)
    gate_full = jnp.dot(routed, both[0], preferred_element_type=jnp.float32)
    up_full = jnp.dot(routed, both[1], preferred_element_type=jnp.float32)
    hidden = (jax.nn.silu(gate_full) * up_full).astype(jnp.bfloat16)
    product = jnp.dot(hidden, down_whole, preferred_element_type=jnp.float32).astype(jnp.bfloat16)
    arrived = lax.all_to_all(
        product.reshape(experts, CAP, width), "ep", split_axis=0, concat_axis=0, tiled=True
    ).reshape(slots, width)
    share = jnp.exp(expert_logit)
    weight = group_weight[:, None] * (share / jnp.sum(share, axis=-1, keepdims=True))
    spread = jnp.where(slot[None, :] == at0[:, None], weight[:, 0:1], 0.0) + jnp.where(
        slot[None, :] == at1[:, None], weight[:, 1:2], 0.0
    )
    high = spread.astype(jnp.bfloat16)
    low = (spread - high.astype(jnp.float32)).astype(jnp.bfloat16)
    mixed = jnp.dot(high, arrived, preferred_element_type=jnp.float32) + jnp.dot(
        low, arrived, preferred_element_type=jnp.float32
    )
    residual = (tokens_f + mixed).astype(jnp.bfloat16)
    pieces = residual.reshape(rows, 4, width // 4).transpose(1, 0, 2)
    sliced = lax.all_to_all(pieces, "tp", split_axis=0, concat_axis=0, tiled=True)
    sliced = sliced.reshape(4 * rows, width // 4).astype(jnp.float32)
    squares = lax.all_gather(jnp.sum(sliced * sliced, axis=-1), "tp", axis=0).sum(axis=0)
    inverse_out = lax.rsqrt(squares / D + EPS)
    return (sliced * inverse_out[:, None] * final_gain.astype(jnp.float32)).astype(jnp.bfloat16)


def solution(mesh):
    placed = (
        P(("ep", "tp"), None),
        P(),
        P(("ep", "tp"), None),
        P(("ep", "tp")),
        P(("ep", "tp"), None),
        P("ep", None, "tp"),
        P("ep", None, "tp"),
        P("ep", "tp", None),
        P("tp"),
    )
    return jax.shard_map(
        local, mesh=mesh, in_specs=placed, out_specs=P("ep", "tp"), check_vma=False
    )
```

profile of v0, /device:TPU:38, one launch (start us, length us, event | category | flops | bytes accessed | tf_op | source)
XLA Modules:
  0.0 317.0 jit_solution(2494651620982889680)
XLA Ops:
  6.5 0.0 all-gather.4.cloned.1.call-start
  6.5 3.1 pad_maximum_fusion
  9.7 0.0 all-gather.4.cloned.1.call-update
  9.7 0.0 copy-done.3
  9.7 0.0 copy-done.2
  9.7 0.2 select_reduce_fusion.1
  10.0 0.0 copy-done
  10.0 0.3 fusion.8
  10.3 3.3 %convolution_convert_fusion = bf16[1024,2048]{1,0:T(8,128)(2,1)} fusion(bf16[256,2048]{1,0:T(8,128)(2,1)S(1)} %copy-done, f32[2048]{0:T(1024)S(1)} %convert_element_type.88, f32[256]{0:T(256)S(1)} %add_rsqrt_fusion.1, s32[256]{0:T(256)S(1)} %get-tuple-element.13, s32[256]{0:T(256)S(1)} %get-tuple-element.14), kind=kOutput, calls=%fused_computation.7 | convolution fusion | flops 1078722560 | bytes 5254144 | tf_op jit(solution)/shard_map/dot_general | solution.py:35
  13.6 11.7 %all-to-all-start = ((bf16[64,16,2048]{2,1,0:T(8,128)(2,1)}), bf16[64,16,2048]{2,1,0:T(8,128)(2,1)}, u32[]{:S(2)}, u32[]{:S(2)}) async-start(bf16[64,16,2048]{2,1,0:T(8,128)(2,1)} %bitcast.43), calls=%async_computation | async-start | bytes 8388608 | tf_op jit(solution)/shard_map/all_to_all | solution.py:36
  25.3 0.0 all-gather.6.cloned.1.call-start
  25.4 0.7 all-gather.6.cloned.1.call-update
  26.1 94.5 %all-to-all-done = bf16[64,16,2048]{2,1,0:T(8,128)(2,1)} async-done(((bf16[64,16,2048]{2,1,0:T(8,128)(2,1)}), bf16[64,16,2048]{2,1,0:T(8,128)(2,1)}, u32[]{:S(2)}, u32[]{:S(2)}) %all-to-all-start) | async-done | bytes 4194336 | tf_op jit(solution)/shard_map/all_to_all | solution.py:36
  120.6 7.6 %fusion = f32[1024,1024]{1,0:T(8,128)S(1)} fusion(bf16[1024,2048]{1,0:T(8,128)(2,1)} %bitcast.9, bf16[2,2048,1024]{2,1,0:T(8,128)(2,1)} %all-gather.4.cloned.1.call-done), kind=kOutput, calls=%fused_computation.1 | convolution fusion | flops 4294967296 | bytes 12582912 | tf_op jit(solution)/shard_map/dot_general | solution.py:41
  128.3 0.0 copy-done.6
  128.3 7.6 %multiply_convert_fusion = bf16[1024,1024]{1,0:T(8,128)(2,1)S(1)} fusion(f32[1024,1024]{1,0:T(8,128)S(1)} %fusion, bf16[1024,2048]{1,0:T(8,128)(2,1)} %bitcast.9, bf16[2,2048,1024]{2,1,0:T(8,128)(2,1)S(1)} %copy-done.6), kind=kOutput, calls=%fused_computation.6 | convolution fusion | flops 4301258752 | bytes 14680064 | tf_op jit(solution)/shard_map/dot_general | solution.py:40
  135.9 18.9 %all-gather.6.cloned.1.call-done = bf16[1,1024,2048]{2,1,0:T(8,128)(2,1)} async-done(((bf16[1,256,2048]{2,1,0:T(8,128)(2,1)}), bf16[1,1024,2048]{2,1,0:T(8,128)(2,1)}) %all-gather.6.cloned.1.call-update) | async-done | bytes 4194320 | tf_op jit(solution)/shard_map/all_gather | solution.py:17
  154.8 8.2 %fusion.4 = bf16[1024,2048]{1,0:T(8,128)(2,1)} fusion(bf16[1024,1024]{1,0:T(8,128)(2,1)S(1)} %multiply_convert_fusion, bf16[1,1024,2048]{2,1,0:T(8,128)(2,1)} %all-gather.6.cloned.1.call-done), kind=kOutput, calls=%fused_computation.8 | convolution fusion | flops 4297064448 | bytes 10485760 | tf_op jit(solution)/shard_map/dot_general | solution.py:43
  163.0 10.8 %all-to-all-start.1 = ((bf16[64,16,2048]{2,1,0:T(8,128)(2,1)}), bf16[64,16,2048]{2,1,0:T(8,128)(2,1)}, u32[]{:S(2)}, u32[]{:S(2)}) async-start(bf16[64,16,2048]{2,1,0:T(8,128)(2,1)} %bitcast.44), calls=%async_computation.1 | async-start | bytes 8388608 | tf_op jit(solution)/shard_map/all_to_all | solution.py:44
  173.8 0.0 copy-done.1
  173.8 0.0 copy-done.5
  173.9 95.1 %all-to-all-done.1 = bf16[64,16,2048]{2,1,0:T(8,128)(2,1)} async-done(((bf16[64,16,2048]{2,1,0:T(8,128)(2,1)}), bf16[64,16,2048]{2,1,0:T(8,128)(2,1)}, u32[]{:S(2)}, u32[]{:S(2)}) %all-to-all-start.1) | async-done | bytes 4194336 | tf_op jit(solution)/shard_map/all_to_all | solution.py:44
  269.0 3.6 %fusion.27 = f32[256,2048]{1,0:T(8,128)S(1)} fusion(bf16[1024,2048]{1,0:T(8,128)(2,1)} %bitcast.14, f32[256]{0:T(256)S(1)} %bitcast.54, s32[256]{0:T(256)S(1)} %bitcast.58, f32[256]{0:T(256)S(1)} %bitcast.52, s32[256]{0:T(256)S(1)} %bitcast.56), kind=kOutput, calls=%fused_computation.40 | convolution fusion | flops 1075314688 | bytes 6295552 | tf_op jit(solution)/shard_map/dot_general | solution.py:54
  272.7 3.7 %fusion.7 = bf16[256,2048]{1,0:T(8,128)(2,1)S(1)} fusion(f32[256,2048]{1,0:T(8,128)S(1)} %fusion.27, bf16[1024,2048]{1,0:T(8,128)(2,1)} %bitcast.14, bf16[256,2048]{1,0:T(8,128)(2,1)S(1)} %copy-done, f32[256]{0:T(256)S(1)} %bitcast.55, s32[256]{0:T(256)S(1)} %bitcast.59, f32[256]{0:T(256)S(1)} %bitcast.53, s32[256]{0:T(256)S(1)} %bitcast.57), kind=kOutput, calls=%fused_computation.13 | convolution fusion | flops 1078198272 | bytes 8392704 | tf_op jit(solution)/shard_map/dot_general | solution.py:54
  276.4 0.0 copy-start.4
  276.4 1.1 copy.19
  277.5 3.5 %all-to-all-start.2 = ((bf16[4,256,512]{2,1,0:T(8,128)(2,1)}), bf16[4,256,512]{2,1,0:T(8,128)(2,1)S(1)}, u32[]{:S(2)}, u32[]{:S(2)}) async-start(bf16[4,256,512]{2,1,0:T(8,128)(2,1)} %bitcast.42), calls=%async_computation.2 | async-start | bytes 2097152 | tf_op jit(solution)/shard_map/all_to_all | solution.py:59
  281.0 0.0 copy-done.4
  281.0 15.5 %all-to-all-done.2 = bf16[4,256,512]{2,1,0:T(8,128)(2,1)S(1)} async-done(((bf16[4,256,512]{2,1,0:T(8,128)(2,1)}), bf16[4,256,512]{2,1,0:T(8,128)(2,1)S(1)}, u32[]{:S(2)}, u32[]{:S(2)}) %all-to-all-start.2) | async-done | bytes 1048608 | tf_op jit(solution)/shard_map/all_to_all | solution.py:59
  296.5 0.3 multiply_reduce_fusion
  296.8 12.0 %all-gather = f32[4,1,1024]{2,1,0:T(1,128)S(1)} all-gather(f32[1,1,1024]{2,1,0:T(1,128)S(1)} %reshape.77), channel_id=1, replica_groups=mesh['ep'=64,'tp'=4] {'tp'}, dimensions={0}, use_global_device_ids=true | all-gather | bytes 20480 | tf_op jit(solution)/shard_map/all_gather | solution.py:61
  308.8 1.3 fusion.12
  (21 shorter events, 0.1 us)
Async XLA Ops:
  6.5 3.2 copy-start.3
  6.5 3.2 %copy-start.2 = (s32[256,2]{0,1:T(2,128)S(1)}, s32[256,2]{0,1:T(2,128)}, u32[]{:S(2)}) copy-start(s32[256,2]{0,1:T(2,128)} %param.11) | copy-start | bytes 6148
  6.5 3.4 %copy-start = (bf16[256,2048]{1,0:T(8,128)(2,1)S(1)}, bf16[256,2048]{1,0:T(8,128)(2,1)}, u32[]{:S(2)}) copy-start(bf16[256,2048]{1,0:T(8,128)(2,1)} %param.9) | copy-start | bytes 3145732
  6.5 114.1 %all-gather.4.cloned.1.call-start = ((), (), s32[]{:S(2)}) async-start(), calls=%async_computation.3 | async-start | bytes 10485760 | tf_op jit(solution)/shard_map/all_gather | solution.py:18
  13.6 107.0 %all-to-all-start = ((bf16[64,16,2048]{2,1,0:T(8,128)(2,1)}), bf16[64,16,2048]{2,1,0:T(8,128)(2,1)}, u32[]{:S(2)}, u32[]{:S(2)}) async-start(bf16[64,16,2048]{2,1,0:T(8,128)(2,1)} %bitcast.43), calls=%async_computation | async-start | bytes 8388608 | tf_op jit(solution)/shard_map/all_to_all | solution.py:36
  25.3 129.5 %all-gather.6.cloned.1.call-start = ((), (), s32[]{:S(2)}) async-start(), calls=%async_computation.4 | async-start | bytes 5242880 | tf_op jit(solution)/shard_map/all_gather | solution.py:17
  120.6 7.7 %copy-start.6 = (bf16[2,2048,1024]{2,1,0:T(8,128)(2,1)S(1)}, bf16[2,2048,1024]{2,1,0:T(8,128)(2,1)}, u32[]{:S(2)}) copy-start(bf16[2,2048,1024]{2,1,0:T(8,128)(2,1)} %all-gather.4.cloned.1.call-done) | copy-start | bytes 25165828
  163.0 10.8 %copy-start.1 = (f32[256,2]{0,1:T(2,128)S(1)}, f32[256,2]{0,1:T(2,128)}, u32[]{:S(2)}) copy-start(f32[256,2]{0,1:T(2,128)} %param.13) | copy-start | bytes 6148
  163.0 10.8 %copy-start.5 = (f32[256]{0:T(256)S(1)}, f32[256]{0:T(256)}, u32[]{:S(2)}) copy-start(f32[256]{0:T(256)} %param.12) | copy-start | bytes 3076
  163.0 106.0 %all-to-all-start.1 = ((bf16[64,16,2048]{2,1,0:T(8,128)(2,1)}), bf16[64,16,2048]{2,1,0:T(8,128)(2,1)}, u32[]{:S(2)}, u32[]{:S(2)}) async-start(bf16[64,16,2048]{2,1,0:T(8,128)(2,1)} %bitcast.44), calls=%async_computation.1 | async-start | bytes 8388608 | tf_op jit(solution)/shard_map/all_to_all | solution.py:44
  276.4 4.6 %copy-start.4 = (bf16[512]{0:T(512)(128)(2,1)S(1)}, bf16[512]{0:T(512)(128)(2,1)}, u32[]{:S(2)}) copy-start(bf16[512]{0:T(512)(128)(2,1)} %param.17) | copy-start | bytes 3076
  277.5 19.0 %all-to-all-start.2 = ((bf16[4,256,512]{2,1,0:T(8,128)(2,1)}), bf16[4,256,512]{2,1,0:T(8,128)(2,1)S(1)}, u32[]{:S(2)}, u32[]{:S(2)}) async-start(bf16[4,256,512]{2,1,0:T(8,128)(2,1)} %bitcast.42), calls=%async_computation.2 | async-start | bytes 2097152 | tf_op jit(solution)/shard_map/all_to_all | solution.py:59
Sparse Core Ops, SparseCore 0:
  9.8 91.9 all-gather.3
  103.6 51.0 all-gather.5
where the time goes:
time: 317 us
  waiting for transfers between devices  225 us (71%)
  matrix products  34.3 us (11%)
  starting transfers between devices  26 us (8%)
  between operations  13.6 us (4%)
  blocking collectives  12 us (4%)
  other arithmetic  5.08 us (2%)
    all_to_all x1, waiting for transfers between devices, local(): lax.all_to_all(product.reshape(experts, CAP, width), 'ep', split_axis=0,...  95.1 us
    all_to_all x1, waiting for transfers between devices, local(): lax.all_to_all(outgoing.reshape(experts, CAP, width), 'ep', split_axis=0,...  94.5 us
    all_gather x1, waiting for transfers between devices, local(): down_whole = lax.all_gather(w_down, 'tp', axis=1, tiled=True)[0]  18.9 us
    all_to_all x1, waiting for transfers between devices, local(): lax.all_to_all(pieces, 'tp', split_axis=0, concat_axis=0, tiled=True)  15.5 us
    all_gather x1, blocking collectives, local(): lax.all_gather(jnp.sum(sliced * sliced, axis=-1), 'tp', axis=0).sum(axis=0)  12 us
    all_to_all x1, starting transfers between devices, local(): lax.all_to_all(outgoing.reshape(experts, CAP, width), 'ep', split_axis=0,...  11.7 us
    all_to_all x1, starting transfers between devices, local(): lax.all_to_all(product.reshape(experts, CAP, width), 'ep', split_axis=0,...  10.8 us
    dot_general x1, matrix products, local(): jnp.dot(hidden, down_whole, preferred_element_type=jnp.float32)  8.2 us
  transfers between devices with their start and end apart: 5, of which 4 were waited for; matrix products, arithmetic and copies ran while one was open for 6% of the time, Pallas kernels for 0%

commit v1 on v0

--- a/solution.py
+++ b/solution.py
@@ -8,13 +8,25 @@
 EPS = 1e-06
 
 
+def collect(value, axis, dim):
+    ways, here, step = (lax.axis_size(axis), lax.axis_index(axis), value.shape[dim])
+    shape = [n * ways if d == dim else n for d, n in enumerate(value.shape)]
+    full = lax.dynamic_update_slice_in_dim(
+        jnp.zeros(shape, value.dtype), value, here * step, axis=dim
+    )
+    for far in range(1, ways):
+        value = lax.ppermute(value, axis, [(d, (d + 1) % ways) for d in range(ways)])
+        full = lax.dynamic_update_slice_in_dim(full, value, (here - far) % ways * step, axis=dim)
+    return full
+
+
 def local(
     tokens, norm_gain, expert_ids, group_weight, expert_logit, w_gate, w_up, w_down, final_gain
 ):
     rows, width = tokens.shape
     experts = lax.axis_size("ep")
     slots = experts * CAP
-    down_whole = lax.all_gather(w_down, "tp", axis=1, tiled=True)[0]
+    down_whole = collect(w_down, "tp", 1)[0]
     both = lax.all_gather(jnp.concatenate((w_gate, w_up), axis=0), "tp", axis=2, tiled=True)
     tokens_f = tokens.astype(jnp.float32)
     inverse_in = lax.rsqrt(jnp.mean(tokens_f * tokens_f, axis=-1, keepdims=True) + EPS)

time: 317 us -> 349 us (1.10)
  waiting for transfers between devices: 225 us -> 243 us
  local copies, waits for them, and re-layouts: 1.12 us -> 10.4 us
    ppermute x0 -> x3, waiting for transfers between devices: none -> 133 us  [collect(): lax.ppermute(value, axis, [(d, (d + 1) % ways) for d in range(ways)])]
    all_to_all x1, waiting for transfers between devices: 94.5 us -> 0.01 us  [local(): lax.all_to_all(outgoing.reshape(experts, CAP, width), 'ep', split_axis=0,...]
    all_gather x1 -> x0, waiting for transfers between devices: 18.9 us -> none  [local(): down_whole = lax.all_gather(w_down, 'tp', axis=1, tiled=True)[0]]
    dot_general x1 -> x0, matrix products: 7.58 us -> none  [local(): gate_full = jnp.dot(routed, both[0], preferred_element_type=jnp.float32)]
    dot_general x1, matrix products: 8.2 us -> 15.4 us  [local(): jnp.dot(hidden, down_whole, preferred_element_type=jnp.float32)]
    dynamic_update_slice x0 -> x4, local copies, waits for them, and re-layouts: none -> 6.8 us  [the longest x3 5.76 us: collect(): lax.dynamic_update_slice_in_dim(full, value, (here - far) % ways * step,...]
  transfers between devices with their start and end apart: 5 -> 7, of which waited for: 4 -> 5; matrix products, arithmetic and copies ran while one was open for 6% -> 4% of each run, Pallas kernels for 0% -> 0%
where the time goes in v1:
time: 349 us
  waiting for transfers between devices  243 us (70%)
  matrix products  36.2 us (10%)
  starting transfers between devices  28.7 us (8%)
  between operations  13.6 us (4%)
  blocking collectives  12 us (3%)
  local copies, waits for them, and re-layouts  10.4 us (3%)
  other arithmetic  5.12 us (1%)
    ppermute x3, waiting for transfers between devices, collect(): lax.ppermute(value, axis, [(d, (d + 1) % ways) for d in range(ways)])  133 us
    all_to_all x1, waiting for transfers between devices, local(): lax.all_to_all(product.reshape(experts, CAP, width), 'ep', split_axis=0,...  95.2 us
    dot_general x1, matrix products, local(): jnp.dot(hidden, down_whole, preferred_element_type=jnp.float32)  15.4 us
    all_to_all x1, waiting for transfers between devices, local(): lax.all_to_all(pieces, 'tp', split_axis=0, concat_axis=0, tiled=True)  15.2 us
    all_gather x1, blocking collectives, local(): lax.all_gather(jnp.sum(sliced * sliced, axis=-1), 'tp', axis=0).sum(axis=0)  12 us
    all_to_all x1, starting transfers between devices, local(): lax.all_to_all(outgoing.reshape(experts, CAP, width), 'ep', split_axis=0,...  11.8 us
    all_to_all x1, starting transfers between devices, local(): lax.all_to_all(product.reshape(experts, CAP, width), 'ep', split_axis=0,...  10.8 us
    dot_general x1, matrix products, local(): up_full = jnp.dot(routed, both[1], preferred_element_type=jnp.float32)  9.89 us
  transfers between devices with their start and end apart: 7, of which 5 were waited for; matrix products, arithmetic and copies ran while one was open for 4% of the time, Pallas kernels for 0%

profile of v1, /device:TPU:38, one launch (start us, length us, event | category | flops | bytes accessed | tf_op | source)
XLA Modules:
  0.0 349.0 jit_solution(15600119221481125319)
XLA Ops:
  6.5 3.2 pad_maximum_fusion
  9.7 0.0 all-gather.3.cloned.1.call-update
  9.7 0.0 copy-done.4
  9.8 0.2 select_reduce_fusion.1
  10.0 0.3 fusion.3
  10.3 3.3 convolution_convert_fusion
  13.7 11.8 %all-to-all-start = ((bf16[64,16,2048]{2,1,0:T(8,128)(2,1)}), bf16[64,16,2048]{2,1,0:T(8,128)(2,1)}, u32[]{:S(2)}, u32[]{:S(2)}) async-start(bf16[64,16,2048]{2,1,0:T(8,128)(2,1)} %bitcast.48), calls=%async_computation | async-start | bytes 8388608 | tf_op jit(solution)/shard_map/all_to_all | solution.py:48
  25.5 1.7 collective-permute-start
  27.2 47.3 %collective-permute-done = bf16[1,256,2048]{2,1,0:T(8,128)(2,1)S(1)} collective-permute-done((bf16[1,256,2048]{2,1,0:T(8,128)(2,1)S(1)}, bf16[1,256,2048]{2,1,0:T(8,128)(2,1)S(1)}, u32[]{:S(2)}, u32[]{:S(2)}) %collective-permute-start) | collective-permute-done | bytes 1048608 | tf_op jit(solution)/shard_map/ppermute | solution.py:18
  74.5 0.1 collective-permute-start.1
  74.5 48.2 %collective-permute-done.1 = bf16[1,256,2048]{2,1,0:T(8,128)(2,1)} collective-permute-done((bf16[1,256,2048]{2,1,0:T(8,128)(2,1)S(1)}, bf16[1,256,2048]{2,1,0:T(8,128)(2,1)}, u32[]{:S(2)}, u32[]{:S(2)}) %collective-permute-start.1) | collective-permute-done | bytes 1048608 | tf_op jit(solution)/shard_map/ppermute | solution.py:18
  122.8 0.0 collective-permute-start.2
  122.8 2.5 squeeze.21
  125.3 1.0 bitcast_dynamic-update-slice_fusion.3
  126.3 1.1 bitcast_dynamic-update-slice_fusion.2
  127.4 2.4 bitcast_dynamic-update-slice_fusion.1
  129.7 37.0 %collective-permute-done.2 = bf16[1,256,2048]{2,1,0:T(8,128)(2,1)} collective-permute-done((bf16[1,256,2048]{2,1,0:T(8,128)(2,1)}, bf16[1,256,2048]{2,1,0:T(8,128)(2,1)}, u32[]{:S(2)}, u32[]{:S(2)}) %collective-permute-start.2) | collective-permute-done | bytes 1048608 | tf_op jit(solution)/shard_map/ppermute | solution.py:18
  166.7 2.3 bitcast_dynamic-update-slice_fusion
  169.1 0.0 all-to-all-done
  169.1 9.9 %fusion = f32[1024,1024]{1,0:T(8,128)} fusion(bf16[1024,2048]{1,0:T(8,128)(2,1)} %bitcast.9, bf16[2,2048,1024]{2,1,0:T(8,128)(2,1)} %all-gather.3.cloned.1.call-done), kind=kOutput, calls=%fused_computation.1 | convolution fusion | flops 4294967296 | bytes 12582912 | tf_op jit(solution)/shard_map/dot_general | solution.py:53
  179.0 15.4 %convolution_convert_fusion.1 = bf16[1024,2048]{1,0:T(8,128)(2,1)} fusion(bf16[1024,2048]{1,0:T(8,128)(2,1)} %bitcast_dynamic-update-slice_fusion, f32[1024,1024]{1,0:T(8,128)} %fusion, bf16[1024,2048]{1,0:T(8,128)(2,1)} %bitcast.9, bf16[2,2048,1024]{2,1,0:T(8,128)(2,1)} %all-gather.3.cloned.1.call-done), kind=kOutput, calls=%fused_computation.6 | convolution fusion | flops 8598323200 | bytes 20971520 | tf_op jit(solution)/shard_map/dot_general | solution.py:55
  194.4 10.8 %all-to-all-start.1 = ((bf16[64,16,2048]{2,1,0:T(8,128)(2,1)}), bf16[64,16,2048]{2,1,0:T(8,128)(2,1)}, u32[]{:S(2)}, u32[]{:S(2)}) async-start(bf16[64,16,2048]{2,1,0:T(8,128)(2,1)} %bitcast.49), calls=%async_computation.1 | async-start | bytes 8388608 | tf_op jit(solution)/shard_map/all_to_all | solution.py:56
  205.3 95.2 %all-to-all-done.1 = bf16[64,16,2048]{2,1,0:T(8,128)(2,1)} async-done(((bf16[64,16,2048]{2,1,0:T(8,128)(2,1)}), bf16[64,16,2048]{2,1,0:T(8,128)(2,1)}, u32[]{:S(2)}, u32[]{:S(2)}) %all-to-all-start.1) | async-done | bytes 4194336 | tf_op jit(solution)/shard_map/all_to_all | solution.py:56
  300.4 3.6 %fusion.22 = f32[256,2048]{1,0:T(8,128)S(1)} fusion(bf16[1024,2048]{1,0:T(8,128)(2,1)} %bitcast.17, f32[256]{0:T(256)S(1)} %bitcast.59, s32[256]{0:T(256)S(1)} %bitcast.63, f32[256]{0:T(256)S(1)} %bitcast.57, s32[256]{0:T(256)S(1)} %bitcast.61), kind=kOutput, calls=%fused_computation.42 | convolution fusion | flops 1075314688 | bytes 6295552 | tf_op jit(solution)/shard_map/dot_general | solution.py:66
  304.1 3.7 %fusion.2 = bf16[256,2048]{1,0:T(8,128)(2,1)S(1)} fusion(f32[256,2048]{1,0:T(8,128)S(1)} %fusion.22, bf16[1024,2048]{1,0:T(8,128)(2,1)} %bitcast.17, bf16[256,2048]{1,0:T(8,128)(2,1)S(1)} %copy-done, f32[256]{0:T(256)S(1)} %bitcast.60, s32[256]{0:T(256)S(1)} %bitcast.64, f32[256]{0:T(256)S(1)} %bitcast.58, s32[256]{0:T(256)S(1)} %bitcast.62), kind=kOutput, calls=%fused_computation.11 | convolution fusion | flops 1078198272 | bytes 8392704 | tf_op jit(solution)/shard_map/dot_general | solution.py:66
  307.8 0.0 copy-start.5
  307.8 1.1 copy.19
  308.9 4.4 %all-to-all-start.2 = ((bf16[4,256,512]{2,1,0:T(8,128)(2,1)}), bf16[4,256,512]{2,1,0:T(8,128)(2,1)S(1)}, u32[]{:S(2)}, u32[]{:S(2)}) async-start(bf16[4,256,512]{2,1,0:T(8,128)(2,1)} %bitcast.47), calls=%async_computation.2 | async-start | bytes 2097152 | tf_op jit(solution)/shard_map/all_to_all | solution.py:71
  313.3 15.2 %all-to-all-done.2 = bf16[4,256,512]{2,1,0:T(8,128)(2,1)S(1)} async-done(((bf16[4,256,512]{2,1,0:T(8,128)(2,1)}), bf16[4,256,512]{2,1,0:T(8,128)(2,1)S(1)}, u32[]{:S(2)}, u32[]{:S(2)}) %all-to-all-start.2) | async-done | bytes 1048608 | tf_op jit(solution)/shard_map/all_to_all | solution.py:71
  328.5 0.3 multiply_reduce_fusion
  328.8 12.0 %all-gather = f32[4,1,1024]{2,1,0:T(1,128)S(1)} all-gather(f32[1,1,1024]{2,1,0:T(1,128)S(1)} %reshape.85), channel_id=1, replica_groups=mesh['ep'=64,'tp'=4] {'tp'}, dimensions={0}, use_global_device_ids=true | all-gather | bytes 20480 | tf_op jit(solution)/shard_map/all_gather | solution.py:73
  340.8 1.3 fusion.7
  (28 shorter events, 0.2 us)
Async XLA Ops:
  6.5 3.2 copy-start.4
  6.5 3.2 copy-start.3
  6.5 3.5 copy-start
  6.5 162.5 %all-gather.3.cloned.1.call-start = ((), (), s32[]{:S(2)}) async-start(), calls=%async_computation.3 | async-start | bytes 10485760 | tf_op jit(solution)/shard_map/all_gather | solution.py:30
  13.7 11.8 %copy-start.1 = (bf16[1,256,2048]{2,1,0:T(8,128)(2,1)S(1)}, bf16[1,256,2048]{2,1,0:T(8,128)(2,1)}, u32[]{:S(2)}) copy-start(bf16[1,256,2048]{2,1,0:T(8,128)(2,1)} %param.16) | copy-start | bytes 3145732
  13.7 155.4 %all-to-all-start = ((bf16[64,16,2048]{2,1,0:T(8,128)(2,1)}), bf16[64,16,2048]{2,1,0:T(8,128)(2,1)}, u32[]{:S(2)}, u32[]{:S(2)}) async-start(bf16[64,16,2048]{2,1,0:T(8,128)(2,1)} %bitcast.48), calls=%async_computation | async-start | bytes 8388608 | tf_op jit(solution)/shard_map/all_to_all | solution.py:48
  25.5 48.9 %collective-permute-start = (bf16[1,256,2048]{2,1,0:T(8,128)(2,1)S(1)}, bf16[1,256,2048]{2,1,0:T(8,128)(2,1)S(1)}, u32[]{:S(2)}, u32[]{:S(2)}) collective-permute-start(bf16[1,256,2048]{2,1,0:T(8,128)(2,1)S(1)} %copy-done.1), channel_id=1, source_target_pairs={{0,1},{1,2},{2,3},{3,0},{4,5},{5,6},{6,7},{7,4},{8,9},{9,10},{10,1... | collective-permute-start | bytes 3145736 | tf_op jit(solution)/shard_map/ppermute | solution.py:18
  74.5 48.3 %collective-permute-start.1 = (bf16[1,256,2048]{2,1,0:T(8,128)(2,1)S(1)}, bf16[1,256,2048]{2,1,0:T(8,128)(2,1)}, u32[]{:S(2)}, u32[]{:S(2)}) collective-permute-start(bf16[1,256,2048]{2,1,0:T(8,128)(2,1)S(1)} %collective-permute-done), channel_id=1, source_target_pairs={{0,1},{1,2},{2,3},{3,0},{4,5},{5,6},{6,7},{7,4},{8,9},{9,10},{10,1... | collective-permute-start | bytes 3145736 | tf_op jit(solution)/shard_map/ppermute | solution.py:18
  122.8 44.0 %collective-permute-start.2 = (bf16[1,256,2048]{2,1,0:T(8,128)(2,1)}, bf16[1,256,2048]{2,1,0:T(8,128)(2,1)}, u32[]{:S(2)}, u32[]{:S(2)}) collective-permute-start(bf16[1,256,2048]{2,1,0:T(8,128)(2,1)} %collective-permute-done.1), channel_id=1, source_target_pairs={{0,1},{1,2},{2,3},{3,0},{4,5},{5,6},{6,7},{7,4},{8,9},{9,10},{10,1... | collective-permute-start | bytes 3145736 | tf_op jit(solution)/shard_map/ppermute | solution.py:18
  194.4 10.8 %copy-start.2 = (f32[256,2]{0,1:T(2,128)S(1)}, f32[256,2]{0,1:T(2,128)}, u32[]{:S(2)}) copy-start(f32[256,2]{0,1:T(2,128)} %param.13) | copy-start | bytes 6148
  194.4 10.9 %copy-start.6 = (f32[256]{0:T(256)S(1)}, f32[256]{0:T(256)}, u32[]{:S(2)}) copy-start(f32[256]{0:T(256)} %param.12) | copy-start | bytes 3076
  194.4 106.1 %all-to-all-start.1 = ((bf16[64,16,2048]{2,1,0:T(8,128)(2,1)}), bf16[64,16,2048]{2,1,0:T(8,128)(2,1)}, u32[]{:S(2)}, u32[]{:S(2)}) async-start(bf16[64,16,2048]{2,1,0:T(8,128)(2,1)} %bitcast.49), calls=%async_computation.1 | async-start | bytes 8388608 | tf_op jit(solution)/shard_map/all_to_all | solution.py:56
  307.8 5.4 %copy-start.5 = (bf16[512]{0:T(512)(128)(2,1)S(1)}, bf16[512]{0:T(512)(128)(2,1)}, u32[]{:S(2)}) copy-start(bf16[512]{0:T(512)(128)(2,1)} %param.17) | copy-start | bytes 3076
  308.9 19.6 %all-to-all-start.2 = ((bf16[4,256,512]{2,1,0:T(8,128)(2,1)}), bf16[4,256,512]{2,1,0:T(8,128)(2,1)S(1)}, u32[]{:S(2)}, u32[]{:S(2)}) async-start(bf16[4,256,512]{2,1,0:T(8,128)(2,1)} %bitcast.47), calls=%async_computation.2 | async-start | bytes 2097152 | tf_op jit(solution)/shard_map/all_to_all | solution.py:71
Sparse Core Ops, SparseCore 0:
  9.9 155.8 all-gather.2
